TPU v7x, 32 devices: a whole 2x2x4 slice. The times are simulated.
32 devices in a mesh: sp: 8 (over z, x), dp: 4 (over y, core).
Axes of the slice: x: 2, y: 2, z: 4, core: 2. Of those that a mesh axis runs over, the one named last changes fastest.
Arguments:
- skip_stream_entering: bfloat16 [4, 1024, 2048], P('dp', 'sp'), may hold values from -6 to 6
- mapped_probe_matrix: bfloat16 [4, 1024, 2048], P('dp', 'sp'), may hold values from -6 to 6
- mapped_lookup_matrix: bfloat16 [4, 1024, 2048], P('dp', 'sp'), may hold values from -6 to 6
- mapped_content_matrix: bfloat16 [4, 1024, 4096], P('dp', 'sp'), may hold values from -6 to 6
- retention_preactivation: bfloat16 [4, 1024, 2048], P('dp', 'sp'), may hold values from -4 to 12
- extra_shrinkage: float32 [4, 16, 1024], P('dp', 'sp'), may hold values from -0.6932 to 0
- attention_group_scale: float32 [4096], replicated, may hold values from 0.1 to 1.9
- final_projection_matrix: bfloat16 [4096, 2048], P(None, 'dp'), may hold values from -0.09375 to 0.09375
- blender_branch_scale: float32 [2048], replicated, may hold values from 0.1 to 1.9
- specialist_prenormal_scale: float32 [2048], replicated, may hold values from 0.1 to 1.9
- specialist_switch_matrix: bfloat16 [32, 2048, 1024], P(('sp', 'dp')), may hold values from -0.125 to 0.125
- specialist_expand_matrix: bfloat16 [32, 2048, 1024], P(('sp', 'dp')), may hold values from -0.125 to 0.125
- specialist_contract_matrix: bfloat16 [32, 1024, 2048], P(('sp', 'dp')), may hold values from -0.1875 to 0.1875
- specialist_branch_scale: float32 [2048], replicated, may hold values from 0.1 to 1.9
- assigned_specialists: int32 [4, 1024, 2], P('dp', 'sp'), may hold values from 0 to 31, all different within a row; in each aligned block of 128 rows (0 to 127, 128 to 255, ..., all dimensions but the last counted through in order) at most 13 rows name the same one
- dispatcher_logits: float32 [4, 1024, 2], P('dp', 'sp'), may hold values from 0.2 to 1
Outputs:
- layer_out: bfloat16 [4, 1024, 2048], P('dp', 'sp')
Inputs may be any that keep to these rules, and one draw needn't show every extreme that they name: `assigned_specialists`: in the rows of one device no expert is named more than 13 times; in every draw some expert reaches 13 on some device.
All inputs are finite; a program needn't handle non-finite values.
Results may differ from a plain program's by a relative error of at most 0.013.
Values may be sent and summed in bfloat16 or wider, within the bound.
A program may use at most 128 MiB of HBM per device.

v0:
```python
import jax
import jax.numpy as jnp
from jax import lax
from jax.sharding import PartitionSpec as P

D = 2048
ATTENTION_GROUPS = 16
KEY_WIDTH = 128
DV = 256
TOP = 2
BLOCK = 64


epsilon = 1e-06
softness_factor = 16.0
highest = lax.Precision.HIGHEST


def rms_scale(values, gain):
    mean_square = jnp.mean(values * values, axis=-1, keepdims=True)
    return values * lax.rsqrt(mean_square + epsilon) * gain


def combine_states(earlier, later):
    return (earlier[0] * later[0], later[0][..., None] * earlier[1] + later[1])


def block_attention(query_f, key_f, value_f, shrink_exponent):
    length_value, head_count, key_dim = query_f.shape
    value_dim = value_f.shape[-1]
    block_count = length_value // BLOCK
    query_blocks = query_f.reshape(block_count, BLOCK, head_count, key_dim)
    key_blocks = key_f.reshape(block_count, BLOCK, head_count, key_dim)
    value_blocks = value_f.reshape(block_count, BLOCK, head_count, value_dim)
    within = jnp.cumsum(shrink_exponent.reshape(block_count, BLOCK, head_count, key_dim), axis=1)
    block_end = within[:, -1]
    lifted = query_blocks * jnp.exp(within)
    lowered = key_blocks * jnp.exp(-within)
    scores = jnp.einsum("nthk,nshk->nhts", lifted, lowered, precision=highest)
    causal = jnp.arange(BLOCK)[:, None] >= jnp.arange(BLOCK)[None, :]
    scores = jnp.where(causal, scores, 0.0)
    inside = jnp.einsum("nhts,nshv->nthv", scores, value_blocks, precision=highest)
    carried_keys = key_blocks * jnp.exp(block_end[:, None] - within)
    updates = jnp.einsum("nshk,nshv->nhkv", carried_keys, value_blocks, precision=highest)
    decays = jnp.exp(block_end)
    total_decay, states = lax.associative_scan(combine_states, (decays, updates), axis=0)
    entering = jnp.concatenate([jnp.zeros_like(states[:1]), states[:-1]], axis=0)
    across = jnp.einsum("nthk,nhkv->nthv", lifted, entering, precision=highest)
    outputs = (inside + across).reshape(length_value, head_count, value_dim)
    offsets = jnp.cumsum(block_end, axis=0) - block_end
    reached = (query_blocks * jnp.exp(within + offsets[:, None])).reshape(
        length_value, head_count, key_dim
    )
    return (outputs, total_decay[-1], states[-1], reached)


def shards(
    skip_stream_entering,
    mapped_probe_matrix,
    mapped_lookup_matrix,
    mapped_content_matrix,
    retention_preactivation,
    extra_shrinkage,
    attention_group_scale,
    final_projection_matrix,
    blender_branch_scale,
    specialist_prenormal_scale,
    specialist_switch_matrix,
    specialist_expand_matrix,
    specialist_contract_matrix,
    specialist_branch_scale,
    assigned_specialists,
    dispatcher_logits,
):
    tok_rows = mapped_probe_matrix.shape[1]
    sp_count = lax.axis_size("sp")
    dp_count = lax.axis_size("dp")
    query_local = mapped_probe_matrix[0].reshape(tok_rows, ATTENTION_GROUPS, KEY_WIDTH)
    key_local = mapped_lookup_matrix[0].reshape(tok_rows, ATTENTION_GROUPS, KEY_WIDTH)
    value_local = mapped_content_matrix[0].reshape(tok_rows, ATTENTION_GROUPS, DV)
    decay_local = retention_preactivation[0].reshape(tok_rows, ATTENTION_GROUPS, KEY_WIDTH)
    arrived = (
        lax.all_to_all(query_local, "sp", split_axis=1, concat_axis=0, tiled=True),
        lax.all_to_all(key_local, "sp", split_axis=1, concat_axis=0, tiled=True),
        lax.all_to_all(value_local, "sp", split_axis=1, concat_axis=0, tiled=True),
        lax.all_to_all(decay_local, "sp", split_axis=1, concat_axis=0, tiled=True),
    )
    query_head, key_head, value_head, head_decay = arrived
    own_heads = query_head.shape[1]
    shrink_exponent = jax.nn.log_sigmoid(head_decay.astype(jnp.float32)) / softness_factor
    shrink_exponent = shrink_exponent + jnp.transpose(extra_shrinkage[0])[:, :, None]
    outputs = block_attention(
        query_head.astype(jnp.float32) * KEY_WIDTH ** (-0.5),
        key_head.astype(jnp.float32),
        value_head.astype(jnp.float32),
        shrink_exponent,
    )[0]
    offset = lax.axis_index("sp") * (own_heads * DV)
    gains = lax.dynamic_slice_in_dim(attention_group_scale, offset, own_heads * DV).reshape(
        own_heads, DV
    )
    normed = rms_scale(outputs, gains).astype(jnp.bfloat16)
    attention_group_result = lax.all_to_all(normed, "sp", split_axis=0, concat_axis=1, tiled=True)
    flat_heads = attention_group_result.reshape(tok_rows, ATTENTION_GROUPS * DV)
    projected = jnp.dot(
        flat_heads,
        lax.all_gather(final_projection_matrix, "dp", axis=1, tiled=True),
        preferred_element_type=jnp.float32,
    ).astype(jnp.bfloat16)
    stream = skip_stream_entering[0].astype(jnp.float32)
    residual = (stream + rms_scale(projected.astype(jnp.float32), blender_branch_scale)).astype(
        jnp.bfloat16
    )
    expert_in = rms_scale(residual.astype(jnp.float32), specialist_prenormal_scale).astype(
        jnp.bfloat16
    )
    expert_total = sp_count * dp_count
    capacity = max(2, 5 * tok_rows * TOP // (3 * expert_total))
    chosen = assigned_specialists[0].reshape(-1)
    pair_total = chosen.shape[0]
    onehot = (chosen[:, None] == jnp.arange(expert_total, dtype=jnp.int32)[None, :]).astype(
        jnp.int32
    )
    ranks = jnp.sum((jnp.cumsum(onehot, axis=0) - onehot) * onehot, axis=1)
    slots = chosen * capacity + ranks
    table = jnp.full((expert_total * capacity,), pair_total, jnp.int32)
    table = table.at[slots].set(jnp.arange(pair_total, dtype=jnp.int32))
    padded = jnp.concatenate([expert_in, jnp.zeros((1, D), jnp.bfloat16)], axis=0)
    outgoing = padded[table // TOP].reshape(expert_total, capacity, D)
    arrived_rows = lax.all_to_all(outgoing, ("sp", "dp"), split_axis=0, concat_axis=0, tiled=True)
    row_block = arrived_rows.reshape(-1, D)
    gate_part = jnp.dot(row_block, specialist_switch_matrix[0], preferred_element_type=jnp.float32)
    up_part = jnp.dot(row_block, specialist_expand_matrix[0], preferred_element_type=jnp.float32)
    hidden_units = (jax.nn.silu(gate_part) * up_part).astype(jnp.bfloat16)
    result = jnp.dot(
        hidden_units, specialist_contract_matrix[0], preferred_element_type=jnp.float32
    )
    returned = lax.all_to_all(
        result.astype(jnp.bfloat16).reshape(arrived_rows.shape),
        ("sp", "dp"),
        split_axis=0,
        concat_axis=0,
        tiled=True,
    )
    flat_back = returned.reshape(expert_total * capacity, D)
    pair_rows = flat_back[slots].reshape(tok_rows, TOP, D)
    weights = dispatcher_logits[0]
    weights = weights / jnp.sum(weights, axis=1, keepdims=True)
    combined = jnp.sum(pair_rows.astype(jnp.float32) * weights[:, :, None], axis=1)
    layer_out = residual.astype(jnp.float32) + rms_scale(combined, specialist_branch_scale)
    return layer_out.astype(jnp.bfloat16)[None]


def solution(mesh):
    return jax.shard_map(
        shards,
        mesh=mesh,
        in_specs=(
            P("dp", "sp", None),
            P("dp", "sp", None),
            P("dp", "sp", None),
            P("dp", "sp", None),
            P("dp", "sp", None),
            P("dp", "sp", None),
            P(),
            P(None, "dp"),
            P(),
            P(),
            P(("sp", "dp"), None, None),
            P(("sp", "dp"), None, None),
            P(("sp", "dp"), None, None),
            P(),
            P("dp", "sp", None),
            P("dp", "sp", None),
        ),
        out_specs=P("dp", "sp", None),
        check_vma=False,
    )
```

profile of v0, /device:TPU:25, one launch (start us, length us, event | category | flops | bytes accessed | tf_op | source)
XLA Modules:
  0.0 355.5 jit_solution(7891554783984080326)
XLA Ops:
  8.6 5.5 %all-to-all-start.1 = ((bf16[128,16,128]{0,2,1:T(8,128)(2,1)}), bf16[128,16,128]{0,2,1:T(8,128)(2,1)S(1)}, u32[]{:S(2)}, u32[]{:S(2)}) async-start(bf16[128,16,128]{0,2,1:T(8,128)(2,1)} %bitcast.6), calls=%async_computation.1 | async-start | bytes 1048576 | tf_op jit(solution)/shard_map/all_to_all | solution.py:86
  15.1 10.7 %all-to-all-done.1 = bf16[128,16,128]{0,2,1:T(8,128)(2,1)S(1)} async-done(((bf16[128,16,128]{0,2,1:T(8,128)(2,1)}), bf16[128,16,128]{0,2,1:T(8,128)(2,1)S(1)}, u32[]{:S(2)}, u32[]{:S(2)}) %all-to-all-start.1) | async-done | bytes 524320 | tf_op jit(solution)/shard_map/all_to_all | solution.py:86
  25.8 6.6 %all-to-all-start.2 = ((bf16[128,16,128]{0,2,1:T(8,128)(2,1)}), bf16[128,16,128]{0,2,1:T(8,128)(2,1)S(1)}, u32[]{:S(2)}, u32[]{:S(2)}) async-start(bf16[128,16,128]{0,2,1:T(8,128)(2,1)} %bitcast.13), calls=%async_computation.2 | async-start | bytes 1048576 | tf_op jit(solution)/shard_map/all_to_all | solution.py:84
  33.4 11.2 %all-to-all-done.2 = bf16[128,16,128]{0,2,1:T(8,128)(2,1)S(1)} async-done(((bf16[128,16,128]{0,2,1:T(8,128)(2,1)}), bf16[128,16,128]{0,2,1:T(8,128)(2,1)S(1)}, u32[]{:S(2)}, u32[]{:S(2)}) %all-to-all-start.2) | async-done | bytes 524320 | tf_op jit(solution)/shard_map/all_to_all | solution.py:84
  44.5 6.1 %all-to-all-start = ((bf16[128,16,128]{0,2,1:T(8,128)(2,1)}), bf16[128,16,128]{0,2,1:T(8,128)(2,1)}, u32[]{:S(2)}, u32[]{:S(2)}) async-start(bf16[128,16,128]{0,2,1:T(8,128)(2,1)} %bitcast.1), calls=%async_computation | async-start | bytes 1048576 | tf_op jit(solution)/shard_map/all_to_all | solution.py:83
  53.9 8.4 %all-to-all-done = bf16[128,16,128]{0,2,1:T(8,128)(2,1)} async-done(((bf16[128,16,128]{0,2,1:T(8,128)(2,1)}), bf16[128,16,128]{0,2,1:T(8,128)(2,1)}, u32[]{:S(2)}, u32[]{:S(2)}) %all-to-all-start) | async-done | bytes 524320 | tf_op jit(solution)/shard_map/all_to_all | solution.py:83
  62.4 6.6 %all-to-all-start.3 = ((bf16[128,16,256]{0,2,1:T(8,128)(2,1)}), bf16[128,16,256]{0,2,1:T(8,128)(2,1)S(1)}, u32[]{:S(2)}, u32[]{:S(2)}) async-start(bf16[128,16,256]{0,2,1:T(8,128)(2,1)} %bitcast.18), calls=%async_computation.3 | async-start | bytes 2097152 | tf_op jit(solution)/shard_map/all_to_all | solution.py:85
  74.8 4.0 %exponential_multiply_fusion = (f32[16,64,2,128]{3,0,1,2:T(8,128)}, f32[16,64,2,128]{3,0,1,2:T(8,128)S(1)}, f32[16,64,2,128]{3,0,1,2:T(8,128)S(1)}) fusion(f32[16,64,2,128]{3,0,1,2:T(8,128)S(1)} %fusion.30, f32[16,64,2,128]{3,1,0,2:T(8,128)} %bitcast.106, f32[16,2,128]{2,0,1:T(8,128)S(1)} %slice_bitcast_fusion, f32[16,64,2,128]{3,1,0,2:T(8,128)} %bitcast.107), kind=kLoop, calls=%fused_computation.49 | loop fusion | flops 1310720 | bytes 6307840 | tf_op jit(solution)/shard_map/mul | solution.py:43
  78.7 3.5 convolution_select_fusion
  82.2 10.6 %all-to-all-done.3 = bf16[128,16,256]{0,2,1:T(8,128)(2,1)S(1)} async-done(((bf16[128,16,256]{0,2,1:T(8,128)(2,1)}), bf16[128,16,256]{0,2,1:T(8,128)(2,1)S(1)}, u32[]{:S(2)}, u32[]{:S(2)}) %all-to-all-start.3) | async-done | bytes 1048608 | tf_op jit(solution)/shard_map/all_to_all | solution.py:85
  93.3 3.7 %fusion.27 = f32[16,2,128,256]{3,2,1,0:T(8,128)S(1)} fusion(f32[16,64,2,128]{3,0,1,2:T(8,128)} %get-tuple-element.7, bf16[16,64,2,256]{3,1,0,2:T(8,128)(2,1)S(1)} %bitcast.97), kind=kOutput, calls=%fused_computation.40 | convolution fusion | flops 805306368 | bytes 6291456 | tf_op jit(solution)/shard_map/nshk,nshv->nhkv/dot_general | solution.py:44
  102.6 4.2 %pad.30 = f32[4,2,128,256]{3,2,1,0:T(8,128)} pad(f32[2,2,128,256]{3,2,1,0:T(8,128)} %pad_add_fusion, f32[]{:T(128)} %constant.27.clone.1), padding=1_0_1x0_0_0x0_0_0x0_0_0 | pad | bytes 1572868 | tf_op jit(solution)/shard_map/pad | solution.py:46
  108.8 4.1 %pad.29 = f32[4,2,128,256]{3,2,1,0:T(8,128)} pad(f32[2,2,128,256]{3,2,1,0:T(8,128)} %pad_maximum_fusion.2, f32[]{:T(128)} %constant.27.clone.1), padding=0_1_1x0_0_0x0_0_0x0_0_0 | pad | bytes 1572868 | tf_op jit(solution)/shard_map/pad | solution.py:46
  112.9 2.8 add.160
  117.7 3.9 %pad.31 = f32[8,2,128,256]{3,2,1,0:T(8,128)S(1)} pad(f32[4,2,128,256]{3,2,1,0:T(8,128)} %pad_maximum_fusion.1, f32[]{:T(128)} %constant.27.clone.1), padding=0_1_1x0_0_0x0_0_0x0_0_0 | pad | bytes 3145732 | tf_op jit(solution)/shard_map/pad | solution.py:46
  121.6 6.6 %pad.32 = f32[8,2,128,256]{3,2,1,0:T(8,128)} pad(f32[4,2,128,256]{3,2,1,0:T(8,128)} %add.160, f32[]{:T(128)} %constant.27.clone.1), padding=1_0_1x0_0_0x0_0_0x0_0_0 | pad | bytes 3145732 | tf_op jit(solution)/shard_map/pad | solution.py:46
  128.2 3.2 add.162
  131.4 11.5 %pad.66 = f32[16,2,128,256]{3,2,1,0:T(8,128)} pad(f32[8,2,128,256]{3,2,1,0:T(8,128)} %add.162, f32[]{:T(128)} %constant.27.clone.1), padding=1_0_1x0_0_0x0_0_0x0_0_0 | pad | bytes 6291460
  146.9 11.5 %pad.44 = f32[15,2,128,256]{3,2,1,0:T(8,128)} pad(f32[8,2,128,256]{3,2,1,0:T(8,128)} %pad_maximum_fusion, f32[]{:T(128)} %constant.27.clone.1), padding=0_0_1x0_0_0x0_0_0x0_0_0 | pad | bytes 6029316 | tf_op jit(solution)/shard_map/slice | solution.py:47
  160.5 2.9 fusion.16.clone.4
  163.5 2.9 multiply_reduce_fusion.1
  169.0 5.8 %all-to-all-start.4 = ((bf16[1024,2,256]{2,1,0:T(2,128)(2,1)}), bf16[1024,2,256]{2,1,0:T(2,128)(2,1)S(1)}, u32[]{:S(2)}, u32[]{:S(2)}) async-start(bf16[1024,2,256]{2,1,0:T(2,128)(2,1)} %copy.206), calls=%async_computation.4 | async-start | bytes 2097152 | tf_op jit(solution)/shard_map/all_to_all | solution.py:103
  177.8 21.2 %all-to-all-done.4 = bf16[1024,2,256]{2,1,0:T(2,128)(2,1)S(1)} async-done(((bf16[1024,2,256]{2,1,0:T(2,128)(2,1)}), bf16[1024,2,256]{2,1,0:T(2,128)(2,1)S(1)}, u32[]{:S(2)}, u32[]{:S(2)}) %all-to-all-start.4) | async-done | bytes 1048608 | tf_op jit(solution)/shard_map/all_to_all | solution.py:103
  200.1 8.3 %multiply_reduce_fusion.3 = (f32[128]{0:T(128)S(1)}, f32[128,2048]{1,0:T(8,128)S(1)}) fusion(bf16[128,4096]{0,1:T(8,128)(2,1)S(1)} %bitcast.99, bf16[4096,2048]{1,0:T(8,128)(2,1)} %all-gather.2.cloned.1.call-done), kind=kOutput, calls=%fused_computation.47 | convolution fusion | flops 2148532224 | bytes 18874880 | tf_op jit(solution)/shard_map/dot_general | solution.py:105
  209.3 3.2 gather_fusion
  214.3 52.0 %all_to_all.67 = bf16[32,13,2048]{2,1,0:T(8,128)(2,1)} all-to-all(bf16[32,13,2048]{2,1,0:T(8,128)(2,1)S(1)} %reshape.176), channel_id=1, replica_groups=mesh['sp'=8,'dp'=4] {'sp','dp'}, dimensions={0} | all-to-all | bytes 3407872 | tf_op jit(solution)/shard_map/all_to_all | solution.py:130
  268.1 5.3 %fusion.4 = f32[416,1024]{1,0:T(8,128)} fusion(bf16[416,2048]{1,0:T(8,128)(2,1)S(1)} %reshape.177, bf16[1,2048,1024]{2,1,0:T(8,128)(2,1)} %param.26), kind=kOutput, calls=%fused_computation.7 | convolution fusion | flops 1744830464 | bytes 7602176 | tf_op jit(solution)/shard_map/dot_general | solution.py:132
  273.5 8.9 %fusion.8 = bf16[416,2048]{1,0:T(8,128)(2,1)} fusion(bf16[1,1024,2048]{2,1,0:T(8,128)(2,1)} %param.28, f32[416,1024]{1,0:T(8,128)} %fusion.4, bf16[416,2048]{1,0:T(8,128)(2,1)S(1)} %reshape.177, bf16[1,2048,1024]{2,1,0:T(8,128)(2,1)} %param.27), kind=kOutput, calls=%fused_computation.12 | convolution fusion | flops 3493068800 | bytes 13500416 | tf_op jit(solution)/shard_map/dot_general | solution.py:135
  282.4 2.8 reshape.178
  285.1 6.2 %all-to-all-start.6 = ((bf16[32,13,2048]{2,1,0:T(8,128)(2,1)}), bf16[32,13,2048]{2,1,0:T(8,128)(2,1)}, u32[]{:S(2)}, u32[]{:S(2)}) async-start(bf16[32,13,2048]{2,1,0:T(8,128)(2,1)} %reshape.178), calls=%async_computation.6 | async-start | bytes 4194304 | tf_op jit(solution)/shard_map/all_to_all | solution.py:138
  291.5 46.2 %all-to-all-done.6 = bf16[32,13,2048]{2,1,0:T(8,128)(2,1)} async-done(((bf16[32,13,2048]{2,1,0:T(8,128)(2,1)}), bf16[32,13,2048]{2,1,0:T(8,128)(2,1)}, u32[]{:S(2)}, u32[]{:S(2)}) %all-to-all-start.6) | async-done | bytes 1703968 | tf_op jit(solution)/shard_map/all_to_all | solution.py:138
  344.3 3.2 multiply_reduce_fusion
  (139 shorter events, 48.4 us)
Async XLA Ops:
  6.5 1.0 copy-start.12
  6.5 193.6 %all-gather.2.cloned.1.call-start = ((), (), s32[]{:S(2)}) async-start(), calls=%async_computation.7 | async-start | bytes 20971520 | tf_op jit(solution)/shard_map/all_gather | solution.py:107
  7.6 6.5 %copy-start.13 = (bf16[1,128,2048]{2,1,0:T(8,128)(2,1)S(1)}, bf16[1,128,2048]{2,1,0:T(8,128)(2,1)}, u32[]{:S(2)}) copy-start(bf16[1,128,2048]{2,1,0:T(8,128)(2,1)} %param.18) | copy-start | bytes 1572868
  7.6 24.8 %copy-start.14 = (bf16[1,128,2048]{2,1,0:T(8,128)(2,1)S(1)}, bf16[1,128,2048]{2,1,0:T(8,128)(2,1)}, u32[]{:S(2)}) copy-start(bf16[1,128,2048]{2,1,0:T(8,128)(2,1)} %param.17) | copy-start | bytes 1572868
  8.6 17.2 %all-to-all-start.1 = ((bf16[128,16,128]{0,2,1:T(8,128)(2,1)}), bf16[128,16,128]{0,2,1:T(8,128)(2,1)S(1)}, u32[]{:S(2)}, u32[]{:S(2)}) async-start(bf16[128,16,128]{0,2,1:T(8,128)(2,1)} %bitcast.6), calls=%async_computation.1 | async-start | bytes 1048576 | tf_op jit(solution)/shard_map/all_to_all | solution.py:86
  14.0 36.6 %copy-start.19 = (f32[1,2,1024]{2,1,0:T(2,128)S(1)}, f32[1,2,1024]{2,1,0:T(2,128)}, u32[]{:S(2)}) copy-start(f32[1,2,1024]{2,1,0:T(2,128)} %param.21) | copy-start | bytes 24580
  14.1 36.7 %copy-start.10 = (bf16[1,128,4096]{2,1,0:T(8,128)(2,1)S(1)}, bf16[1,128,4096]{2,1,0:T(8,128)(2,1)}, u32[]{:S(2)}) copy-start(bf16[1,128,4096]{2,1,0:T(8,128)(2,1)} %param.19) | copy-start | bytes 3145732
  25.8 18.7 %all-to-all-start.2 = ((bf16[128,16,128]{0,2,1:T(8,128)(2,1)}), bf16[128,16,128]{0,2,1:T(8,128)(2,1)S(1)}, u32[]{:S(2)}, u32[]{:S(2)}) async-start(bf16[128,16,128]{0,2,1:T(8,128)(2,1)} %bitcast.13), calls=%async_computation.2 | async-start | bytes 1048576 | tf_op jit(solution)/shard_map/all_to_all | solution.py:84
  44.5 8.4 %copy-start.9 = (bf16[128,16,128]{0,2,1:T(8,128)(2,1)}, bf16[128,16,128]{0,2,1:T(8,128)(2,1)S(1)}, u32[]{:S(2)}) copy-start(bf16[128,16,128]{0,2,1:T(8,128)(2,1)S(1)} %all-to-all-done.2) | copy-start | bytes 1572868
  44.5 17.8 %all-to-all-start = ((bf16[128,16,128]{0,2,1:T(8,128)(2,1)}), bf16[128,16,128]{0,2,1:T(8,128)(2,1)}, u32[]{:S(2)}, u32[]{:S(2)}) async-start(bf16[128,16,128]{0,2,1:T(8,128)(2,1)} %bitcast.1), calls=%async_computation | async-start | bytes 1048576 | tf_op jit(solution)/shard_map/all_to_all | solution.py:83
  62.4 30.4 %all-to-all-start.3 = ((bf16[128,16,256]{0,2,1:T(8,128)(2,1)}), bf16[128,16,256]{0,2,1:T(8,128)(2,1)S(1)}, u32[]{:S(2)}, u32[]{:S(2)}) async-start(bf16[128,16,256]{0,2,1:T(8,128)(2,1)} %bitcast.18), calls=%async_computation.3 | async-start | bytes 2097152 | tf_op jit(solution)/shard_map/all_to_all | solution.py:85
  93.3 3.7 %copy-start.2 = (bf16[8,128,2,256]{3,1,0,2:T(8,128)(2,1)}, bf16[8,128,2,256]{3,1,0,2:T(8,128)(2,1)S(1)}, u32[]{:S(2)}) copy-start(bf16[8,128,2,256]{3,1,0,2:T(8,128)(2,1)S(1)} %copy.193) | copy-start | bytes 3145732
  97.0 1.9 copy-start
  99.9 1.0 copy-start.6
  101.1 0.7 copy-start.8
  112.9 2.8 copy-start.4
  112.9 2.8 copy-start.5
  115.7 1.0 copy-start.11
  142.9 2.5 slice-start
  146.8 11.5 %copy-start.3 = (bf16[8,128,2,256]{3,1,0,2:T(8,128)(2,1)S(1)}, bf16[8,128,2,256]{3,1,0,2:T(8,128)(2,1)}, u32[]{:S(2)}) copy-start(bf16[8,128,2,256]{3,1,0,2:T(8,128)(2,1)} %copy-done.2) | copy-start | bytes 3145732
  146.9 11.5 %copy-start.7 = (f32[16,2,64,64]{3,2,1,0:T(8,128)S(1)}, f32[16,2,64,64]{3,2,1,0:T(8,128)}, u32[]{:S(2)}) copy-start(f32[16,2,64,64]{3,2,1,0:T(8,128)} %convolution_select_fusion) | copy-start | bytes 1572868
  158.3 2.2 copy-start.1
  166.9 7.9 %copy-start.20 = (s32[1,128,2]{1,2,0:T(2,128)S(1)}, s32[1,128,2]{1,2,0:T(2,128)}, u32[]{:S(2)}) copy-start(s32[1,128,2]{1,2,0:T(2,128)} %param.30) | copy-start | bytes 3076
  169.0 30.0 %all-to-all-start.4 = ((bf16[1024,2,256]{2,1,0:T(2,128)(2,1)}), bf16[1024,2,256]{2,1,0:T(2,128)(2,1)S(1)}, u32[]{:S(2)}, u32[]{:S(2)}) async-start(bf16[1024,2,256]{2,1,0:T(2,128)(2,1)} %copy.206), calls=%async_computation.4 | async-start | bytes 2097152 | tf_op jit(solution)/shard_map/all_to_all | solution.py:103
  200.1 8.3 %copy-start.15 = (bf16[1,128,2048]{2,1,0:T(8,128)(2,1)S(1)}, bf16[1,128,2048]{2,1,0:T(8,128)(2,1)}, u32[]{:S(2)}) copy-start(bf16[1,128,2048]{2,1,0:T(8,128)(2,1)} %param.16) | copy-start | bytes 1572868
  200.1 8.3 %copy-start.16 = (f32[2048]{0:T(1024)S(1)}, f32[2048]{0:T(1024)}, u32[]{:S(2)}) copy-start(f32[2048]{0:T(1024)} %param.24) | copy-start | bytes 24580
  208.4 0.7 copy-start.17
  285.1 6.2 %copy-start.21 = (f32[1,128,2]{1,2,0:T(2,128)S(1)}, f32[1,128,2]{1,2,0:T(2,128)}, u32[]{:S(2)}) copy-start(f32[1,128,2]{1,2,0:T(2,128)} %param.31) | copy-start | bytes 3076
  285.1 52.6 %all-to-all-start.6 = ((bf16[32,13,2048]{2,1,0:T(8,128)(2,1)}), bf16[32,13,2048]{2,1,0:T(8,128)(2,1)}, u32[]{:S(2)}, u32[]{:S(2)}) async-start(bf16[32,13,2048]{2,1,0:T(8,128)(2,1)} %reshape.178), calls=%async_computation.6 | async-start | bytes 4194304 | tf_op jit(solution)/shard_map/all_to_all | solution.py:138
  344.3 3.3 copy-start.18
Sparse Core Ops, SparseCore 0:
  8.9 107.2 all-gather.1
where the time goes:
time: 361 us; the launch traced here: 356 us
  waiting for transfers between devices  109 us (30%)
  local copies, waits for them, and re-layouts  78.8 us (22%)
  blocking collectives  52 us (14%)
  starting transfers between devices  36.7 us (10%)
  matrix products  33.5 us (9%)
  other arithmetic  31.6 us (9%)
  between operations  13.9 us (4%)
    all_to_all x1, blocking collectives, shards(): lax.all_to_all(outgoing, ('sp', 'dp'), split_axis=0, concat_axis=0, tiled...  52 us
    all_to_all x1, waiting for transfers between devices, shards(): lax.all_to_all(result.astype(jnp.bfloat16).reshape(arrived_rows.shape), (...  46.2 us
    unnamed x50, local copies, waits for them, and re-layouts  21.6 us
    all_to_all x1, waiting for transfers between devices, shards(): lax.all_to_all(normed, 'sp', split_axis=0, concat_axis=1, tiled=True)  21.2 us
    pad x4, local copies, waits for them, and re-layouts, block_attention(): lax.associative_scan(combine_states, (decays, updates), axis=0)  18.7 us
    slice x1, local copies, waits for them, and re-layouts, block_attention(): states[:-1]  11.5 us
    all_to_all x1, waiting for transfers between devices, shards(): lax.all_to_all(key_local, 'sp', split_axis=1, concat_axis=0, tiled=True)  11.2 us
    all_to_all x1, waiting for transfers between devices, shards(): lax.all_to_all(decay_local, 'sp', split_axis=1, concat_axis=0, tiled=True)  10.7 us
  transfers between devices with their start and end apart: 7, of which 6 were waited for; matrix products, arithmetic and copies ran while one was open for 27% of the time, Pallas kernels for 0%

commit v1 on v0

v1 whole, which is shorter than its diff:
```python
import jax
import jax.numpy as jnp
from jax import lax
from jax.experimental import pallas as pl
from jax.experimental.pallas import tpu as pltpu
from jax.sharding import PartitionSpec as P

D = 2048
KEY_WIDTH = 128
DV = 256
TOP = 2
BLOCK = 64


epsilon = 1e-06
softness_factor = 16.0
highest = lax.Precision.HIGHEST


def rms_scale(values, gain):
    mean_square = jnp.mean(values * values, axis=-1, keepdims=True)
    return values * lax.rsqrt(mean_square + epsilon) * gain


def local_kernel(q_ref, k_ref, v_ref, g_ref, e_ref, o_ref, r_ref, u_ref):
    rows = q_ref.shape[0]
    g = g_ref[...].astype(jnp.float32)
    logs = (jnp.minimum(g, 0.0) - jnp.log(1.0 + jnp.exp(-jnp.abs(g)))) / softness_factor
    row = lax.broadcasted_iota(jnp.int32, (rows, rows), 0)
    col = lax.broadcasted_iota(jnp.int32, (rows, rows), 1)
    causal = row >= col
    extra = jnp.sum(jnp.where(causal, e_ref[0], 0.0), axis=1, keepdims=True)
    within = extra + jnp.dot(
        causal.astype(jnp.float32), logs, precision=highest, preferred_element_type=jnp.float32
    )
    middle = within[rows // 2 - 1 : rows // 2]
    end = within[rows - 1 : rows]
    q = q_ref[...].astype(jnp.float32) * KEY_WIDTH ** (-0.5)
    k = k_ref[...].astype(jnp.float32)
    v = v_ref[...]
    lifted = (q * jnp.exp(within - middle)).astype(jnp.bfloat16)
    lowered = (k * jnp.exp(middle - within)).astype(jnp.bfloat16)
    scores = lax.dot_general(
        lifted, lowered, (((1,), (1,)), ((), ())), preferred_element_type=jnp.float32
    )
    scores = jnp.where(causal, scores, 0.0).astype(jnp.bfloat16)
    o_ref[...] = jnp.dot(scores, v, preferred_element_type=jnp.float32)
    r_ref[...] = (q * jnp.exp(within)).astype(jnp.bfloat16)
    carried = (k * jnp.exp(end - within)).astype(jnp.bfloat16)
    u_ref[0] = lax.dot_general(
        v, carried, (((0,), (0,)), ((), ())), preferred_element_type=jnp.float32
    ).astype(jnp.bfloat16)


def scan_kernel(u_ref, d_ref, s_ref):
    count = u_ref.shape[0]
    decay = jnp.exp(d_ref[0])
    state = jnp.zeros(u_ref.shape[2:], jnp.float32)
    for i in range(count):
        s_ref[i, 0] = state.astype(jnp.bfloat16)
        if i < count - 1:
            state = state * decay[i : i + 1] + u_ref[i, 0].astype(jnp.float32)


def finish_kernel(o_ref, r_ref, s_ref, gain_ref, out_ref):
    mixed = o_ref[...] + lax.dot_general(
        r_ref[...], s_ref[0], (((1,), (1,)), ((), ())), preferred_element_type=jnp.float32
    )
    out_ref[...] = rms_scale(mixed, gain_ref[...]).astype(jnp.bfloat16)


def linear_attention(query, key, value, gate, extra_shrinkage, gains):
    rows, width = query.shape
    heads = width // KEY_WIDTH
    sp_count = lax.axis_size("sp")
    own = extra_shrinkage.shape[0]
    logs = jnp.sum(jax.nn.log_sigmoid(gate.astype(jnp.float32)), axis=0) / softness_factor
    spans = jnp.transpose(extra_shrinkage.reshape(own, sp_count, rows), (1, 0, 2))
    small = jnp.concatenate([spans, logs.reshape(sp_count, own, KEY_WIDTH)], axis=2)
    small = lax.all_to_all(small, "sp", split_axis=0, concat_axis=0, tiled=True)
    extra = small[:, :, :rows].reshape(heads, 1, rows)
    decays = jnp.transpose(small[:, :, rows:] + jnp.sum(spans, axis=2)[:, :, None], (1, 0, 2))
    narrow = pl.BlockSpec((rows, KEY_WIDTH), lambda h: (0, h))
    wide = pl.BlockSpec((rows, DV), lambda h: (0, h))
    state = pl.BlockSpec((1, DV, KEY_WIDTH), lambda h: (h, 0, 0))
    inside, reached, updates = pl.pallas_call(
        local_kernel,
        grid=(heads,),
        in_specs=[narrow, narrow, wide, narrow, pl.BlockSpec((1, 1, rows), lambda h: (h, 0, 0))],
        out_specs=[wide, narrow, state],
        out_shape=[
            jax.ShapeDtypeStruct((rows, heads * DV), jnp.float32),
            jax.ShapeDtypeStruct((rows, width), jnp.bfloat16),
            jax.ShapeDtypeStruct((heads, DV, KEY_WIDTH), jnp.bfloat16),
        ],
        name="local",
    )(query, key, value, gate, extra)
    gathered = lax.all_to_all(updates, "sp", split_axis=0, concat_axis=0, tiled=True)
    stack = pl.BlockSpec((sp_count, 1, DV, KEY_WIDTH), lambda h: (0, h, 0, 0))
    entering = pl.pallas_call(
        scan_kernel,
        grid=(own,),
        in_specs=[stack, pl.BlockSpec((1, sp_count, KEY_WIDTH), lambda h: (h, 0, 0))],
        out_specs=stack,
        out_shape=jax.ShapeDtypeStruct((sp_count, own, DV, KEY_WIDTH), jnp.bfloat16),
        name="scan",
    )(gathered.reshape(sp_count, own, DV, KEY_WIDTH), decays)
    entering = lax.all_to_all(
        entering.reshape(updates.shape), "sp", split_axis=0, concat_axis=0, tiled=True
    )
    return pl.pallas_call(
        finish_kernel,
        grid=(heads,),
        in_specs=[wide, narrow, state, pl.BlockSpec((1, DV), lambda h: (0, h))],
        out_specs=wide,
        out_shape=jax.ShapeDtypeStruct((rows, heads * DV), jnp.bfloat16),
        name="finish",
    )(inside, reached, entering, gains.reshape(1, heads * DV))


def shards(
    skip_stream_entering,
    mapped_probe_matrix,
    mapped_lookup_matrix,
    mapped_content_matrix,
    retention_preactivation,
    extra_shrinkage,
    attention_group_scale,
    final_projection_matrix,
    blender_branch_scale,
    specialist_prenormal_scale,
    specialist_switch_matrix,
    specialist_expand_matrix,
    specialist_contract_matrix,
    specialist_branch_scale,
    assigned_specialists,
    dispatcher_logits,
):
    tok_rows = mapped_probe_matrix.shape[1]
    sp_count = lax.axis_size("sp")
    dp_count = lax.axis_size("dp")
    flat_heads = linear_attention(
        mapped_probe_matrix[0],
        mapped_lookup_matrix[0],
        mapped_content_matrix[0],
        retention_preactivation[0],
        extra_shrinkage[0],
        attention_group_scale,
    )
    projected = jnp.dot(
        flat_heads,
        lax.all_gather(final_projection_matrix, "dp", axis=1, tiled=True),
        preferred_element_type=jnp.float32,
    ).astype(jnp.bfloat16)
    stream = skip_stream_entering[0].astype(jnp.float32)
    residual = (stream + rms_scale(projected.astype(jnp.float32), blender_branch_scale)).astype(
        jnp.bfloat16
    )
    expert_in = rms_scale(residual.astype(jnp.float32), specialist_prenormal_scale).astype(
        jnp.bfloat16
    )
    expert_total = sp_count * dp_count
    capacity = max(2, 5 * tok_rows * TOP // (3 * expert_total))
    chosen = assigned_specialists[0].reshape(-1)
    pair_total = chosen.shape[0]
    onehot = (chosen[:, None] == jnp.arange(expert_total, dtype=jnp.int32)[None, :]).astype(
        jnp.int32
    )
    ranks = jnp.sum((jnp.cumsum(onehot, axis=0) - onehot) * onehot, axis=1)
    slots = chosen * capacity + ranks
    table = jnp.full((expert_total * capacity,), pair_total, jnp.int32)
    table = table.at[slots].set(jnp.arange(pair_total, dtype=jnp.int32))
    padded = jnp.concatenate([expert_in, jnp.zeros((1, D), jnp.bfloat16)], axis=0)
    outgoing = padded[table // TOP].reshape(expert_total, capacity, D)
    arrived_rows = lax.all_to_all(outgoing, ("sp", "dp"), split_axis=0, concat_axis=0, tiled=True)
    row_block = arrived_rows.reshape(-1, D)
    gate_part = jnp.dot(row_block, specialist_switch_matrix[0], preferred_element_type=jnp.float32)
    up_part = jnp.dot(row_block, specialist_expand_matrix[0], preferred_element_type=jnp.float32)
    hidden_units = (jax.nn.silu(gate_part) * up_part).astype(jnp.bfloat16)
    result = jnp.dot(
        hidden_units, specialist_contract_matrix[0], preferred_element_type=jnp.float32
    )
    returned = lax.all_to_all(
        result.astype(jnp.bfloat16).reshape(arrived_rows.shape),
        ("sp", "dp"),
        split_axis=0,
        concat_axis=0,
        tiled=True,
    )
    flat_back = returned.reshape(expert_total * capacity, D)
    pair_rows = flat_back[slots].reshape(tok_rows, TOP, D)
    weights = dispatcher_logits[0]
    weights = weights / jnp.sum(weights, axis=1, keepdims=True)
    combined = jnp.sum(pair_rows.astype(jnp.float32) * weights[:, :, None], axis=1)
    layer_out = residual.astype(jnp.float32) + rms_scale(combined, specialist_branch_scale)
    return layer_out.astype(jnp.bfloat16)[None]


def solution(mesh):
    return jax.shard_map(
        shards,
        mesh=mesh,
        in_specs=(
            P("dp", "sp", None),
            P("dp", "sp", None),
            P("dp", "sp", None),
            P("dp", "sp", None),
            P("dp", "sp", None),
            P("dp", "sp", None),
            P(),
            P(None, "dp"),
            P(),
            P(),
            P(("sp", "dp"), None, None),
            P(("sp", "dp"), None, None),
            P(("sp", "dp"), None, None),
            P(),
            P("dp", "sp", None),
            P("dp", "sp", None),
        ),
        out_specs=P("dp", "sp", None),
        check_vma=False,
    )
```

time: 361 us -> 276 us (0.76)
  local copies, waits for them, and re-layouts: 78.8 us -> 21.8 us
  Pallas kernels: 0 us -> 27.5 us
  other arithmetic: 31.6 us -> 7.16 us
  starting transfers between devices: 36.7 us -> 19.1 us
  matrix products: 33.5 us -> 22.7 us
  waiting for transfers between devices: 109 us -> 100 us
  blocking collectives: 52 us -> 58.7 us
    pallas_call x0 -> x3, Pallas kernels: none -> 27.5 us  [the longest x1 14.1 us: linear_attention(): pl.pallas_call(local_kernel, grid=(heads,), in_specs=[narrow, narrow, wid...]
    all_to_all x5 -> x2, waiting for transfers between devices: 62.1 us -> 43.1 us  [the longest x1 22.1 us: linear_attention(): lax.all_to_all(updates, 'sp', split_axis=0, concat_axis=0, tiled=True)]
    unnamed x50 -> x21, local copies, waits for them, and re-layouts: 21.6 us -> 2.69 us
    pad x4 -> x0, local copies, waits for them, and re-layouts: 18.7 us -> none  [block_attention(): lax.associative_scan(combine_states, (decays, updates), axis=0)]
    all_to_all x5 -> x2, starting transfers between devices: 30.5 us -> 12.8 us  [the longest x1 6.61 us: linear_attention(): lax.all_to_all(entering.reshape(updates.shape), 'sp', split_axis=0, conca...]
    slice x19 -> x2, local copies, waits for them, and re-layouts: 12.5 us -> 0.78 us  [the longest x1 0.6 us: linear_attention(): small[:, :, rows:] + jnp.sum(spans, axis=2)[:, :, None]]
    dot_general x4 -> x0, matrix products: 11 us -> none  [the longest x1 3.67 us: block_attention(): jnp.einsum('nshk,nshv->nhkv', carried_keys, value_blocks, precision=highest)]
    add x9 -> x0, other arithmetic: 10.9 us -> none  [the longest x3 6.83 us: block_attention(): lax.associative_scan(combine_states, (decays, updates), axis=0)]
  transfers between devices with their start and end apart: 7 -> 4, of which waited for: 6 -> 4; matrix products, arithmetic and copies ran while one was open for 27% -> 2% of each run, Pallas kernels for 0% -> 10%
where the time goes in v1:
time: 276 us; the launch traced here: 271 us
  waiting for transfers between devices  100 us (36%)
  blocking collectives  58.7 us (21%)
  Pallas kernels  27.5 us (10%)
  matrix products  22.7 us (8%)
  local copies, waits for them, and re-layouts  21.8 us (8%)
  starting transfers between devices  19.1 us (7%)
  between operations  13.6 us (5%)
  other arithmetic  7.16 us (3%)
    all_to_all x1, blocking collectives, shards(): lax.all_to_all(outgoing, ('sp', 'dp'), split_axis=0, concat_axis=0, tiled...  50.8 us
    all_to_all x1, waiting for transfers between devices, shards(): lax.all_to_all(result.astype(jnp.bfloat16).reshape(arrived_rows.shape), (...  46.4 us
    all_to_all x1, waiting for transfers between devices, linear_attention(): lax.all_to_all(updates, 'sp', split_axis=0, concat_axis=0, tiled=True)  22.1 us
    all_to_all x1, waiting for transfers between devices, linear_attention(): lax.all_to_all(entering.reshape(updates.shape), 'sp', split_axis=0, conca...  21 us
    pallas_call x1, Pallas kernels, linear_attention(): pl.pallas_call(local_kernel, grid=(heads,), in_specs=[narrow, narrow, wid...  14.1 us
    pallas_call x1, Pallas kernels, linear_attention(): pl.pallas_call(finish_kernel, grid=(heads,), in_specs=[wide, narrow, stat...  11.3 us
    all_gather x1, waiting for transfers between devices, shards(): lax.all_gather(final_projection_matrix, 'dp', axis=1, tiled=True)  10.1 us
    dot_general x1, matrix products, shards(): jnp.dot(hidden_units, specialist_contract_matrix[0], preferred_element_ty...  8.9 us
  transfers between devices with their start and end apart: 4, of which 4 were waited for; matrix products, arithmetic and copies ran while one was open for 2% of the time, Pallas kernels for 10%

profile of v1, /device:TPU:25, one launch (start us, length us, event | category | flops | bytes accessed | tf_op | source)
XLA Modules:
  0.0 270.9 jit_solution(8282700063777762340)
XLA Ops:
  6.5 0.7 all-gather.2.cloned.1.call-update
  7.6 0.7 fusion.16
  8.3 7.9 %all_to_all.25 = f32[8,2,256]{2,1,0:T(2,128)S(1)} all-to-all(f32[8,2,256]{2,1,0:T(2,128)S(1)} %pad_maximum_fusion), channel_id=1, replica_groups=mesh['sp'=8,'dp'=4] {'sp'}, dimensions={0} | all-to-all | bytes 32768 | tf_op jit(solution)/shard_map/all_to_all | solution.py:80
  16.2 0.6 fusion.32
  16.8 14.1 %local.1 = (f32[128,4096]{1,0:T(8,128)}, bf16[128,2048]{1,0:T(8,128)(2,1)}, bf16[16,256,128]{2,1,0:T(8,128)(2,1)}) custom-call(bf16[128,2048]{1,0:T(8,128)(2,1)} %bitcast.69, bf16[128,2048]{1,0:T(8,128)(2,1)} %bitcast.70, bf16[128,4096]{1,0:T(8,128)(2,1)} %bitcast.68, bf16[128,2048]{1,0:T(8,128)(2,1)} %bitcast.71, f32[16,1,128]{2,1,0:T(1,128)} %bitcast.72), custom_call_target="tpu_custom_call" | custom-call | tf_op jit(solution)/shard_map/local/pallas_call | solution.py:86
  30.9 6.2 %all-to-all-start.1 = ((bf16[16,256,128]{2,1,0:T(8,128)(2,1)}), bf16[16,256,128]{2,1,0:T(8,128)(2,1)S(1)}, u32[]{:S(2)}, u32[]{:S(2)}) async-start(bf16[16,256,128]{2,1,0:T(8,128)(2,1)} %get-tuple-element.10), calls=%async_computation.1 | async-start | bytes 2097152 | tf_op jit(solution)/shard_map/all_to_all | solution.py:98
  37.3 0.7 fusion.25.d_ref
  38.0 22.1 %all-to-all-done.1 = bf16[16,256,128]{2,1,0:T(8,128)(2,1)S(1)} async-done(((bf16[16,256,128]{2,1,0:T(8,128)(2,1)}), bf16[16,256,128]{2,1,0:T(8,128)(2,1)S(1)}, u32[]{:S(2)}, u32[]{:S(2)}) %all-to-all-start.1) | async-done | bytes 1048608 | tf_op jit(solution)/shard_map/all_to_all | solution.py:98
  60.1 1.0 copy-done
  61.1 2.1 scan.1
  63.2 6.6 %all-to-all-start.2 = ((bf16[16,256,128]{2,1,0:T(8,128)(2,1)}), bf16[16,256,128]{2,1,0:T(8,128)(2,1)S(1)}, u32[]{:S(2)}, u32[]{:S(2)}) async-start(bf16[16,256,128]{2,1,0:T(8,128)(2,1)} %bitcast.66), calls=%async_computation.2 | async-start | bytes 2097152 | tf_op jit(solution)/shard_map/all_to_all | solution.py:108
  70.2 0.6 reduce-window.6
  71.4 1.4 scatter_custom_fusion
  72.9 21.0 %all-to-all-done.2.s_ref = bf16[16,256,128]{2,1,0:T(8,128)(2,1)S(1)} async-done(((bf16[16,256,128]{2,1,0:T(8,128)(2,1)}), bf16[16,256,128]{2,1,0:T(8,128)(2,1)S(1)}, u32[]{:S(2)}, u32[]{:S(2)}) %all-to-all-start.2) | async-done | bytes 1048608 | tf_op jit(solution)/shard_map/all_to_all | solution.py:108
  93.9 1.0 copy-done.1
  94.8 11.3 %finish.1 = bf16[128,4096]{1,0:T(8,128)(2,1)} custom-call(f32[128,4096]{1,0:T(8,128)} %get-tuple-element.8.o_ref, bf16[128,2048]{1,0:T(8,128)(2,1)} %get-tuple-element.9.r_ref, bf16[16,256,128]{2,1,0:T(8,128)(2,1)} %copy-done.1, f32[1,4096]{1,0:T(1,128)} %bitcast.75), custom_call_target="tpu_custom_call" | custom-call | tf_op jit(solution)/shard_map/finish/pallas_call | solution.py:111
  106.1 10.1 %all-gather.2.cloned.1.call-done = bf16[4096,2048]{1,0:T(8,128)(2,1)} async-done(((bf16[4096,512]{1,0:T(8,128)(2,1)}), bf16[4096,2048]{1,0:T(8,128)(2,1)}) %all-gather.2.cloned.1.call-update) | async-done | bytes 16777232 | tf_op jit(solution)/shard_map/all_gather | solution.py:152
  116.2 8.5 %multiply_reduce_fusion.2 = (f32[128]{0:T(128)S(1)}, f32[128,2048]{1,0:T(8,128)S(1)}) fusion(bf16[128,4096]{1,0:T(8,128)(2,1)} %finish.1, bf16[4096,2048]{1,0:T(8,128)(2,1)} %all-gather.2.cloned.1.call-done), kind=kOutput, calls=%fused_computation.26 | convolution fusion | flops 2148532224 | bytes 18874880 | tf_op jit(solution)/shard_map/dot_general | solution.py:150
  125.7 3.2 %gather_fusion = bf16[416,2048]{1,0:T(8,128)(2,1)} fusion(bf16[129,2048]{1,0:T(8,128)(2,1)S(1)} %concatenate.7, s32[1024]{0:T(1024)S(1)} %pad_clamp_fusion.1), kind=kCustom, calls=%fused_computation | custom fusion | bytes 3409536 | tf_op jit(solution)/shard_map/gather | solution.py:174
  128.9 1.8 reshape.132
  130.6 50.8 %all_to_all.26 = bf16[32,13,2048]{2,1,0:T(8,128)(2,1)} all-to-all(bf16[32,13,2048]{2,1,0:T(8,128)(2,1)S(1)} %reshape.132), channel_id=1, replica_groups=mesh['sp'=8,'dp'=4] {'sp','dp'}, dimensions={0} | all-to-all | bytes 3407872 | tf_op jit(solution)/shard_map/all_to_all | solution.py:175
  181.4 1.8 reshape.133
  183.3 5.3 %fusion.4 = f32[416,1024]{1,0:T(8,128)} fusion(bf16[416,2048]{1,0:T(8,128)(2,1)S(1)} %reshape.133, bf16[1,2048,1024]{2,1,0:T(8,128)(2,1)} %param.26), kind=kOutput, calls=%fused_computation.7 | convolution fusion | flops 1744830464 | bytes 7602176 | tf_op jit(solution)/shard_map/dot_general | solution.py:177
  188.6 8.9 %fusion.6 = bf16[416,2048]{1,0:T(8,128)(2,1)} fusion(bf16[1,1024,2048]{2,1,0:T(8,128)(2,1)} %param.28, f32[416,1024]{1,0:T(8,128)} %fusion.4, bf16[416,2048]{1,0:T(8,128)(2,1)S(1)} %reshape.133, bf16[1,2048,1024]{2,1,0:T(8,128)(2,1)} %param.27), kind=kOutput, calls=%fused_computation.10 | convolution fusion | flops 3493068800 | bytes 13500416 | tf_op jit(solution)/shard_map/dot_general | solution.py:180
  197.5 2.8 %reshape.134 = bf16[32,13,2048]{2,1,0:T(8,128)(2,1)} reshape(bf16[416,2048]{1,0:T(8,128)(2,1)} %fusion.6) | data formatting | bytes 3407872 | tf_op jit(solution)/shard_map/reshape | solution.py:184
  200.3 6.3 %all-to-all-start.4 = ((bf16[32,13,2048]{2,1,0:T(8,128)(2,1)}), bf16[32,13,2048]{2,1,0:T(8,128)(2,1)}, u32[]{:S(2)}, u32[]{:S(2)}) async-start(bf16[32,13,2048]{2,1,0:T(8,128)(2,1)} %reshape.134), calls=%async_computation.4 | async-start | bytes 4194304 | tf_op jit(solution)/shard_map/all_to_all | solution.py:183
  206.7 46.4 %all-to-all-done.4 = bf16[32,13,2048]{2,1,0:T(8,128)(2,1)} async-done(((bf16[32,13,2048]{2,1,0:T(8,128)(2,1)}), bf16[32,13,2048]{2,1,0:T(8,128)(2,1)}, u32[]{:S(2)}, u32[]{:S(2)}) %all-to-all-start.4) | async-done | bytes 1703968 | tf_op jit(solution)/shard_map/all_to_all | solution.py:183
  253.1 1.8 reshape.135
  255.0 2.3 gather_fusion.1
  257.3 2.4 reshape.137
  259.7 3.2 %multiply_reduce_fusion = f32[128,2048]{1,0:T(8,128)S(1)} fusion(f32[128,2,2048]{2,1,0:T(2,128)S(1)} %reshape.137, f32[128,2]{1,0:T(8,128)S(1)} %copy.40), kind=kLoop, calls=%fused_computation.13 | loop fusion | flops 786432 | bytes 3146752 | tf_op jit(solution)/shard_map/reduce_sum | solution.py:194
  263.0 1.0 fusion.20
  (49 shorter events, 2.7 us)
Async XLA Ops:
  6.5 1.0 copy-start.2
  6.5 1.7 copy-start.4
  6.5 109.7 %all-gather.2.cloned.1.call-start = ((), (), s32[]{:S(2)}) async-start(), calls=%async_computation.5 | async-start | bytes 20971520 | tf_op jit(solution)/shard_map/all_gather | solution.py:152
  30.9 29.2 %all-to-all-start.1 = ((bf16[16,256,128]{2,1,0:T(8,128)(2,1)}), bf16[16,256,128]{2,1,0:T(8,128)(2,1)S(1)}, u32[]{:S(2)}, u32[]{:S(2)}) async-start(bf16[16,256,128]{2,1,0:T(8,128)(2,1)} %get-tuple-element.10), calls=%async_computation.1 | async-start | bytes 2097152 | tf_op jit(solution)/shard_map/all_to_all | solution.py:98
  60.1 1.0 copy-start
  61.1 8.7 %copy-start.8 = (s32[1,128,2]{1,2,0:T(2,128)S(1)}, s32[1,128,2]{1,2,0:T(2,128)}, u32[]{:S(2)}) copy-start(s32[1,128,2]{1,2,0:T(2,128)} %param.30) | copy-start | bytes 3076
  63.2 30.7 %all-to-all-start.2 = ((bf16[16,256,128]{2,1,0:T(8,128)(2,1)}), bf16[16,256,128]{2,1,0:T(8,128)(2,1)S(1)}, u32[]{:S(2)}, u32[]{:S(2)}) async-start(bf16[16,256,128]{2,1,0:T(8,128)(2,1)} %bitcast.66), calls=%async_computation.2 | async-start | bytes 2097152 | tf_op jit(solution)/shard_map/all_to_all | solution.py:108
  93.9 1.0 copy-start.1
  106.1 18.7 %copy-start.3 = (bf16[1,128,2048]{2,1,0:T(8,128)(2,1)S(1)}, bf16[1,128,2048]{2,1,0:T(8,128)(2,1)}, u32[]{:S(2)}) copy-start(bf16[1,128,2048]{2,1,0:T(8,128)(2,1)} %param.16) | copy-start | bytes 1572868
  106.1 18.7 %copy-start.5 = (f32[2048]{0:T(1024)S(1)}, f32[2048]{0:T(1024)}, u32[]{:S(2)}) copy-start(f32[2048]{0:T(1024)} %param.24) | copy-start | bytes 24580
  124.7 0.7 copy-start.6
  200.3 6.3 %copy-start.9 = (f32[1,128,2]{1,2,0:T(2,128)S(1)}, f32[1,128,2]{1,2,0:T(2,128)}, u32[]{:S(2)}) copy-start(f32[1,128,2]{1,2,0:T(2,128)} %param.31) | copy-start | bytes 3076
  200.3 52.8 %all-to-all-start.4 = ((bf16[32,13,2048]{2,1,0:T(8,128)(2,1)}), bf16[32,13,2048]{2,1,0:T(8,128)(2,1)}, u32[]{:S(2)}, u32[]{:S(2)}) async-start(bf16[32,13,2048]{2,1,0:T(8,128)(2,1)} %reshape.134), calls=%async_computation.4 | async-start | bytes 4194304 | tf_op jit(solution)/shard_map/all_to_all | solution.py:183
  259.7 3.3 %copy-start.7 = (f32[2048]{0:T(1024)S(1)}, f32[2048]{0:T(1024)}, u32[]{:S(2)}) copy-start(f32[2048]{0:T(1024)} %param.29) | copy-start | bytes 24580
Sparse Core Ops, SparseCore 0:
  8.9 107.2 all-gather.1

commit v2 on v1

--- a/solution.py
+++ b/solution.py
@@ -118,6 +118,129 @@
     )(inside, reached, entering, gains.reshape(1, heads * DV))
 
 
+PLANES = 4
+LANES = 128
+MESH = pl.DeviceIdType.MESH
+
+
+def expert_kernel(
+    out_ref, gate_hbm, up_hbm, down_hbm, ret_ref, recv, res, gate_w, up_w, down_w,
+    weight_sem, send_sem, recv_sem, back_sem, ret_sem,
+):
+    dp_count = lax.axis_size("dp")
+    total, cap, segments, lanes = out_ref.shape
+    per = total // PLANES
+    me = lax.axis_index("sp") * dp_count + lax.axis_index("dp")
+    plane, place = me // per, lax.rem(me, per)
+
+    def where_is(peer):
+        return (peer // dp_count, lax.rem(peer, dp_count))
+
+    weights = [
+        pltpu.make_async_copy(source.at[0], target, weight_sem.at[i])
+        for i, (source, target) in enumerate(
+            ((gate_hbm, gate_w), (up_hbm, up_w), (down_hbm, down_w))
+        )
+    ]
+    for copy in weights:
+        copy.start()
+    barrier = pltpu.get_barrier_semaphore()
+
+    @pl.loop(1, total)
+    def _(i):
+        peer = lax.rem(me + i, total)
+        pl.semaphore_signal(barrier, inc=1, device_id=where_is(peer), device_id_type=MESH)
+
+    pl.semaphore_wait(barrier, total - 1)
+
+    @pl.loop(1, total)
+    def _(i):
+        peer = lax.rem(plane + i, PLANES) * per + lax.rem(place + i // PLANES, per)
+        pltpu.make_async_remote_copy(
+            src_ref=out_ref.at[peer],
+            dst_ref=recv.at[me],
+            send_sem=send_sem,
+            recv_sem=recv_sem.at[plane],
+            device_id=where_is(peer),
+            device_id_type=MESH,
+        ).start()
+
+    pltpu.make_async_copy(out_ref.at[me], recv.at[me], recv_sem.at[plane]).start()
+    for copy in weights:
+        copy.wait()
+
+    @pl.loop(0, PLANES)
+    def _(step):
+        group = lax.rem(plane + step, PLANES)
+        base = group * per
+        block = recv.at[pl.ds(base, per)]
+        pltpu.make_async_copy(block, block, recv_sem.at[group]).wait()
+        rows = block[...].reshape(per * cap, segments * lanes)
+        gate_part = jnp.dot(rows, gate_w[...], preferred_element_type=jnp.float32)
+        up_part = jnp.dot(rows, up_w[...], preferred_element_type=jnp.float32)
+        hidden = (jax.nn.silu(gate_part) * up_part).astype(jnp.bfloat16)
+        result = jnp.dot(hidden, down_w[...], preferred_element_type=jnp.float32)
+        res[pl.ds(base, per)] = result.astype(jnp.bfloat16).reshape(per, cap, segments, lanes)
+
+        @pl.loop(0, per)
+        def _(j):
+            peer = base + lax.rem(place + j, per)
+
+            @pl.when(peer != me)
+            def _():
+                pltpu.make_async_remote_copy(
+                    src_ref=res.at[peer],
+                    dst_ref=ret_ref.at[me],
+                    send_sem=back_sem,
+                    recv_sem=ret_sem,
+                    device_id=where_is(peer),
+                    device_id_type=MESH,
+                ).start()
+
+            @pl.when(peer == me)
+            def _():
+                pltpu.make_async_copy(res.at[me], ret_ref.at[me], ret_sem).start()
+
+    pltpu.make_async_copy(ret_ref, ret_ref, ret_sem).wait()
+    sent = out_ref.at[pl.ds(0, total - 1)]
+    pltpu.make_async_copy(sent, sent, send_sem).wait()
+    answered = res.at[pl.ds(0, total - 1)]
+    pltpu.make_async_copy(answered, answered, back_sem).wait()
+
+
+def routed_experts(outgoing, gate_weight, up_weight, down_weight):
+    buffer = pltpu.VMEM(outgoing.shape, jnp.bfloat16)
+    weights = [pltpu.VMEM(w.shape[1:], jnp.bfloat16) for w in (gate_weight, up_weight, down_weight)]
+    vmem = pl.BlockSpec(memory_space=pltpu.VMEM)
+    anywhere = pl.BlockSpec(memory_space=pl.ANY)
+    row_count = outgoing.shape[0] * outgoing.shape[1]
+    return pl.pallas_call(
+        expert_kernel,
+        in_specs=[vmem, anywhere, anywhere, anywhere],
+        out_specs=vmem,
+        out_shape=jax.ShapeDtypeStruct(outgoing.shape, jnp.bfloat16),
+        scratch_shapes=[
+            buffer,
+            buffer,
+            *weights,
+            pltpu.SemaphoreType.DMA((3,)),
+            pltpu.SemaphoreType.DMA,
+            pltpu.SemaphoreType.DMA((PLANES,)),
+            pltpu.SemaphoreType.DMA,
+            pltpu.SemaphoreType.DMA,
+        ],
+        compiler_params=pltpu.CompilerParams(
+            collective_id=0, has_side_effects=True, vmem_limit_bytes=56 * 1024 * 1024
+        ),
+        cost_estimate=pl.CostEstimate(
+            flops=6 * row_count * D * gate_weight.shape[2],
+            bytes_accessed=6 * D * gate_weight.shape[2],
+            transcendentals=0,
+        ),
+        name="experts",
+    )(outgoing, gate_weight, up_weight, down_weight)
+
+
 def shards(
     skip_stream_entering,
     mapped_probe_matrix,
@@ -170,28 +293,19 @@
     slots = chosen * capacity + ranks
     table = jnp.full((expert_total * capacity,), pair_total, jnp.int32)
     table = table.at[slots].set(jnp.arange(pair_total, dtype=jnp.int32))
+    segments = D // LANES
     padded = jnp.concatenate([expert_in, jnp.zeros((1, D), jnp.bfloat16)], axis=0)
-    outgoing = padded[table // TOP].reshape(expert_total, capacity, D)
-    arrived_rows = lax.all_to_all(outgoing, ("sp", "dp"), split_axis=0, concat_axis=0, tiled=True)
-    row_block = arrived_rows.reshape(-1, D)
-    gate_part = jnp.dot(row_block, specialist_switch_matrix[0], preferred_element_type=jnp.float32)
-    up_part = jnp.dot(row_block, specialist_expand_matrix[0], preferred_element_type=jnp.float32)
-    hidden_units = (jax.nn.silu(gate_part) * up_part).astype(jnp.bfloat16)
-    result = jnp.dot(
-        hidden_units, specialist_contract_matrix[0], preferred_element_type=jnp.float32
-    )
-    returned = lax.all_to_all(
-        result.astype(jnp.bfloat16).reshape(arrived_rows.shape),
-        ("sp", "dp"),
-        split_axis=0,
-        concat_axis=0,
-        tiled=True,
-    )
-    flat_back = returned.reshape(expert_total * capacity, D)
-    pair_rows = flat_back[slots].reshape(tok_rows, TOP, D)
+    padded = padded.reshape(tok_rows + 1, segments, LANES)
+    outgoing = padded[table // TOP].reshape(expert_total, capacity, segments, LANES)
+    returned = routed_experts(
+        outgoing, specialist_switch_matrix, specialist_expand_matrix, specialist_contract_matrix
+    )
+    flat_back = returned.reshape(expert_total * capacity, segments, LANES)
+    pair_rows = flat_back[slots].reshape(tok_rows, TOP, segments, LANES)
     weights = dispatcher_logits[0]
     weights = weights / jnp.sum(weights, axis=1, keepdims=True)
-    combined = jnp.sum(pair_rows.astype(jnp.float32) * weights[:, :, None], axis=1)
+    combined = jnp.sum(pair_rows.astype(jnp.float32) * weights[:, :, None, None], axis=1)
+    combined = combined.reshape(tok_rows, D)
     layer_out = residual.astype(jnp.float32) + rms_scale(combined, specialist_branch_scale)
     return layer_out.astype(jnp.bfloat16)[None]
 

time: 276 us -> 245 us (0.89); the launches traced: 271 us -> 243 us
  Pallas kernels: 27.5 us -> 130 us
  blocking collectives: 58.7 us -> 7.92 us
  waiting for transfers between devices: 100 us -> 53.8 us
  matrix products: 22.7 us -> 8.52 us
  local copies, waits for them, and re-layouts: 21.8 us -> 10.7 us
  starting transfers between devices: 19.1 us -> 12.8 us
    pallas_call x0 -> x1, Pallas kernels: none -> 103 us  [routed_experts(): pl.pallas_call(expert_kernel, in_specs=[vmem, anywhere, anywhere, anywher...]
    all_to_all x1 -> x0, blocking collectives: 50.8 us -> none  [shards(): lax.all_to_all(outgoing, ('sp', 'dp'), split_axis=0, concat_axis=0, tiled...]
    all_to_all x1 -> x0, waiting for transfers between devices: 46.4 us -> none  [shards(): lax.all_to_all(result.astype(jnp.bfloat16).reshape(arrived_rows.shape), (...]
    dot_general x2 -> x0, matrix products: 14.2 us -> none  [the longest x1 8.9 us: shards(): jnp.dot(hidden_units, specialist_contract_matrix[0], preferred_element_ty...]
    reshape x4 -> x1, local copies, waits for them, and re-layouts: 8.24 us -> 0.04 us  [shards(): padded = padded.reshape(tok_rows + 1, segments, LANES)]
    all_to_all x1 -> x0, starting transfers between devices: 6.29 us -> none  [shards(): lax.all_to_all(result.astype(jnp.bfloat16).reshape(arrived_rows.shape), (...]
    reduce_sum x1, other arithmetic: 3.16 us -> 0.34 us  [shards(): jnp.sum(pair_rows.astype(jnp.float32) * weights[:, :, None, None], axis=1)]
  transfers between devices with their start and end apart: 4 -> 3, of which waited for: 4 -> 3; matrix products, arithmetic and copies ran while one was open for 2% -> 2% of each run, Pallas kernels for 10% -> 11%
where the time goes in v2:
time: 245 us; the launch traced here: 243 us
  Pallas kernels  130 us (53%)
  waiting for transfers between devices  53.8 us (22%)
  between operations  13.6 us (6%)
  starting transfers between devices  12.8 us (5%)
  local copies, waits for them, and re-layouts  10.7 us (4%)
  matrix products  8.52 us (3%)
  blocking collectives  7.92 us (3%)
  other arithmetic  5.51 us (2%)
    pallas_call x1, Pallas kernels, routed_experts(): pl.pallas_call(expert_kernel, in_specs=[vmem, anywhere, anywhere, anywher...  103 us
    all_to_all x1, waiting for transfers between devices, linear_attention(): lax.all_to_all(updates, 'sp', split_axis=0, concat_axis=0, tiled=True)  22.1 us
    all_to_all x1, waiting for transfers between devices, linear_attention(): lax.all_to_all(entering.reshape(updates.shape), 'sp', split_axis=0, conca...  20.8 us
    pallas_call x1, Pallas kernels, linear_attention(): pl.pallas_call(local_kernel, grid=(heads,), in_specs=[narrow, narrow, wid...  14.1 us
    pallas_call x1, Pallas kernels, linear_attention(): pl.pallas_call(finish_kernel, grid=(heads,), in_specs=[wide, narrow, stat...  11.3 us
    all_gather x1, waiting for transfers between devices, shards(): lax.all_gather(final_projection_matrix, 'dp', axis=1, tiled=True)  10.1 us
    dot_general x1, matrix products, shards(): jnp.dot(flat_heads, lax.all_gather(final_projection_matrix, 'dp', axis=1,...  8.52 us
    all_to_all x1, blocking collectives, linear_attention(): small = lax.all_to_all(small, 'sp', split_axis=0, concat_axis=0, tiled=True)  7.92 us
  transfers between devices with their start and end apart: 3, of which 3 were waited for; matrix products, arithmetic and copies ran while one was open for 2% of the time, Pallas kernels for 11%

profile of v2, /device:TPU:25, one launch (start us, length us, event | category | flops | bytes accessed | tf_op | source)
XLA Modules:
  0.0 243.2 jit_solution(15309042954803100786)
XLA Ops:
  6.5 0.7 all-gather.2.cloned.1.call-update
  7.3 0.3 copy-done.2
  7.6 0.7 fusion.6
  8.3 7.9 %all_to_all.15 = f32[8,2,256]{2,1,0:T(2,128)S(1)} all-to-all(f32[8,2,256]{2,1,0:T(2,128)S(1)} %pad_maximum_fusion), channel_id=1, replica_groups=mesh['sp'=8,'dp'=4] {'sp'}, dimensions={0} | all-to-all | bytes 32768 | tf_op jit(solution)/shard_map/all_to_all | solution.py:80
  16.2 0.6 fusion.20
  16.8 14.1 %local.1 = (f32[128,4096]{1,0:T(8,128)}, bf16[128,2048]{1,0:T(8,128)(2,1)}, bf16[16,256,128]{2,1,0:T(8,128)(2,1)}) custom-call(bf16[128,2048]{1,0:T(8,128)(2,1)} %bitcast.74, bf16[128,2048]{1,0:T(8,128)(2,1)} %bitcast.75, bf16[128,4096]{1,0:T(8,128)(2,1)} %bitcast.72, bf16[128,2048]{1,0:T(8,128)(2,1)} %bitcast.76, f32[16,1,128]{2,1,0:T(1,128)} %bitcast.77), custom_call_target="tpu_custom_call" | custom-call | tf_op jit(solution)/shard_map/local/pallas_call | solution.py:86
  30.9 6.2 %all-to-all-start.1 = ((bf16[16,256,128]{2,1,0:T(8,128)(2,1)}), bf16[16,256,128]{2,1,0:T(8,128)(2,1)S(1)}, u32[]{:S(2)}, u32[]{:S(2)}) async-start(bf16[16,256,128]{2,1,0:T(8,128)(2,1)} %get-tuple-element.10), calls=%async_computation.1 | async-start | bytes 2097152 | tf_op jit(solution)/shard_map/all_to_all | solution.py:98
  37.3 0.7 fusion.14.d_ref
  38.0 22.1 %all-to-all-done.1 = bf16[16,256,128]{2,1,0:T(8,128)(2,1)S(1)} async-done(((bf16[16,256,128]{2,1,0:T(8,128)(2,1)}), bf16[16,256,128]{2,1,0:T(8,128)(2,1)S(1)}, u32[]{:S(2)}, u32[]{:S(2)}) %all-to-all-start.1) | async-done | bytes 1048608 | tf_op jit(solution)/shard_map/all_to_all | solution.py:98
  60.1 1.0 copy-done
  61.1 2.1 scan.1
  63.2 6.6 %all-to-all-start.2 = ((bf16[16,256,128]{2,1,0:T(8,128)(2,1)}), bf16[16,256,128]{2,1,0:T(8,128)(2,1)S(1)}, u32[]{:S(2)}, u32[]{:S(2)}) async-start(bf16[16,256,128]{2,1,0:T(8,128)(2,1)} %bitcast.67), calls=%async_computation.2 | async-start | bytes 2097152 | tf_op jit(solution)/shard_map/all_to_all | solution.py:108
  69.9 0.1 eq.29
  70.1 0.1 eq.25
  70.2 0.6 reduce-window.6
  70.8 0.2 slice_reduce_fusion
  71.2 0.1 mul.97
  71.6 1.4 scatter_custom_fusion
  73.0 20.8 %all-to-all-done.2.s_ref = bf16[16,256,128]{2,1,0:T(8,128)(2,1)S(1)} async-done(((bf16[16,256,128]{2,1,0:T(8,128)(2,1)}), bf16[16,256,128]{2,1,0:T(8,128)(2,1)S(1)}, u32[]{:S(2)}, u32[]{:S(2)}) %all-to-all-start.2) | async-done | bytes 1048608 | tf_op jit(solution)/shard_map/all_to_all | solution.py:108
  93.9 1.0 copy-done.1
  94.9 11.3 %finish.1 = bf16[128,4096]{1,0:T(8,128)(2,1)} custom-call(f32[128,4096]{1,0:T(8,128)} %get-tuple-element.8.o_ref, bf16[128,2048]{1,0:T(8,128)(2,1)} %get-tuple-element.9.r_ref, bf16[16,256,128]{2,1,0:T(8,128)(2,1)} %copy-done.1, f32[1,4096]{1,0:T(1,128)} %bitcast.80), custom_call_target="tpu_custom_call" | custom-call | tf_op jit(solution)/shard_map/finish/pallas_call | solution.py:111
  106.1 10.1 %all-gather.2.cloned.1.call-done = bf16[4096,2048]{1,0:T(8,128)(2,1)} async-done(((bf16[4096,512]{1,0:T(8,128)(2,1)}), bf16[4096,2048]{1,0:T(8,128)(2,1)}) %all-gather.2.cloned.1.call-update) | async-done | bytes 16777232 | tf_op jit(solution)/shard_map/all_gather | solution.py:275
  116.2 8.5 %multiply_reduce_fusion.1 = (f32[128]{0:T(128)S(1)}, f32[128,2048]{1,0:T(8,128)S(1)}) fusion(bf16[128,4096]{1,0:T(8,128)(2,1)} %finish.1, bf16[4096,2048]{1,0:T(8,128)(2,1)} %all-gather.2.cloned.1.call-done), kind=kOutput, calls=%fused_computation.21 | convolution fusion | flops 2148532224 | bytes 18874880 | tf_op jit(solution)/shard_map/dot_general | solution.py:273
  124.8 0.4 fusion.2
  125.2 0.3 copy-done.6
  125.5 0.2 fusion.4
  125.9 2.6 %gather_fusion = bf16[416,16,128]{2,1,0:T(8,128)(2,1)} fusion(bf16[129,16,128]{2,1,0:T(8,128)(2,1)S(1)} %slice.23, s32[1024]{0:T(1024)S(1)} %pad_clamp_fusion.1), kind=kCustom, calls=%fused_computation | custom fusion | bytes 3409536 | tf_op jit(solution)/shard_map/gather | solution.py:299
  128.5 102.8 %experts.1 = bf16[32,13,16,128]{3,2,1,0:T(8,128)(2,1)} custom-call(bf16[32,13,16,128]{3,2,1,0:T(8,128)(2,1)} %bitcast.71, bf16[1,2048,1024]{2,1,0:T(8,128)(2,1)} %gate_hbm.1, bf16[1,2048,1024]{2,1,0:T(8,128)(2,1)} %up_hbm.1, bf16[1,1024,2048]{2,1,0:T(8,128)(2,1)} %down_hbm.1), custom_call_target="tpu_custom_call" | custom-call | flops 5234491392 | bytes 12582912 | tf_op jit(solution)/shard_map/experts/pallas_call | solution.py:217
  231.3 2.3 gather_fusion.1
  233.6 0.3 fusion.1
  234.0 1.0 multiply_reduce_fusion
  235.0 1.3 fusion.9
  (42 shorter events, 1.0 us)
Async XLA Ops:
  6.5 1.0 copy-start.2
  6.5 1.7 copy-start.4
  6.5 109.7 %all-gather.2.cloned.1.call-start = ((), (), s32[]{:S(2)}) async-start(), calls=%async_computation.3 | async-start | bytes 20971520 | tf_op jit(solution)/shard_map/all_gather | solution.py:275
  30.9 29.2 %all-to-all-start.1 = ((bf16[16,256,128]{2,1,0:T(8,128)(2,1)}), bf16[16,256,128]{2,1,0:T(8,128)(2,1)S(1)}, u32[]{:S(2)}, u32[]{:S(2)}) async-start(bf16[16,256,128]{2,1,0:T(8,128)(2,1)} %get-tuple-element.10), calls=%async_computation.1 | async-start | bytes 2097152 | tf_op jit(solution)/shard_map/all_to_all | solution.py:98
  60.1 1.0 copy-start
  61.1 8.8 %copy-start.8 = (s32[1,128,2]{1,2,0:T(2,128)S(1)}, s32[1,128,2]{1,2,0:T(2,128)}, u32[]{:S(2)}) copy-start(s32[1,128,2]{1,2,0:T(2,128)} %param.30) | copy-start | bytes 3076
  61.1 10.3 %copy-start.9 = (f32[1,128,2]{1,2,0:T(2,128)S(1)}, f32[1,128,2]{1,2,0:T(2,128)}, u32[]{:S(2)}) copy-start(f32[1,128,2]{1,2,0:T(2,128)} %param.31) | copy-start | bytes 3076
  63.2 30.7 %all-to-all-start.2 = ((bf16[16,256,128]{2,1,0:T(8,128)(2,1)}), bf16[16,256,128]{2,1,0:T(8,128)(2,1)S(1)}, u32[]{:S(2)}, u32[]{:S(2)}) async-start(bf16[16,256,128]{2,1,0:T(8,128)(2,1)} %bitcast.67), calls=%async_computation.2 | async-start | bytes 2097152 | tf_op jit(solution)/shard_map/all_to_all | solution.py:108
  93.9 1.0 copy-start.1
  106.1 18.7 %copy-start.3 = (bf16[1,128,2048]{2,1,0:T(8,128)(2,1)S(1)}, bf16[1,128,2048]{2,1,0:T(8,128)(2,1)}, u32[]{:S(2)}) copy-start(bf16[1,128,2048]{2,1,0:T(8,128)(2,1)} %param.16) | copy-start | bytes 1572868
  106.1 18.7 %copy-start.5 = (f32[2048]{0:T(1024)S(1)}, f32[2048]{0:T(1024)}, u32[]{:S(2)}) copy-start(f32[2048]{0:T(1024)} %param.24) | copy-start | bytes 24580
  124.7 0.7 copy-start.6
  233.6 1.4 copy-start.7
Sparse Core Ops, SparseCore 0:
  8.9 107.2 all-gather.1
